TPU v7x, 32 devices: a whole 2x2x4 slice. The times are simulated.
32 devices in a mesh: sp: 16 (over z, y, x), tp: 2 (over core).
Axes of the slice: x: 2, y: 2, z: 4, core: 2. Of those that a mesh axis runs over, the one named last changes fastest.
Arguments:
- resid: bfloat16 [3072, 2048], P('sp'), may hold values from -6 to 6
- query: bfloat16 [3072, 2048], P('sp', 'tp'), may hold values from -6 to 6
- key: bfloat16 [3072, 1024], P('sp', 'tp'), may hold values from -6 to 6
- value: bfloat16 [3072, 1024], P('sp', 'tp'), may hold values from -6 to 6
- q_gain: float32 [128], replicated, may hold values from 0.3 to 5, as said below
- k_gain: float32 [128], replicated, may hold values from 0.3 to 5, as said below
- out_weight: bfloat16 [2048, 2048], P('tp'), may hold values from -0.125 to 0.125
- norm_gain: float32 [2048], replicated, may hold values from 0.1 to 1.9
- gate_weight: bfloat16 [2048, 5632], P('sp', 'tp'), may hold values from -0.125 to 0.125
- up_weight: bfloat16 [2048, 5632], P('sp', 'tp'), may hold values from -0.125 to 0.125
- down_weight: bfloat16 [5632, 2048], P('tp', 'sp'), may hold values from -0.078125 to 0.078125
Outputs:
- mixed: bfloat16 [3072, 2048], P(('sp', 'tp'))
Inputs may be any that keep to these rules, and one draw needn't show every extreme that they name: `q_gain`: positive gains. `k_gain`: positive gains.
All inputs are finite; a program needn't handle non-finite values.
Results may differ from a plain program's by a relative error of at most 0.012.
The roundings to bfloat16 on the way count: a program that leaves them out, or rounds other values in their place, can miss the bound.
Values may be sent and summed in bfloat16 or wider, within the bound.
A program may use at most 128 MiB of HBM per device.

v0:
```python
import jax
import jax.numpy as jnp
from jax import lax
from jax.sharding import PartitionSpec as P

GRID_W = 64
EPSILON = 1e-06


def rotate(values, positions):
    dim_size = values.shape[-1]
    half_dim = dim_size // 2
    quarter = half_dim // 2
    inverse = 10000.0 ** (-jnp.arange(quarter, dtype=jnp.float32) / quarter)
    outputs = []
    for axis_pos, coords in enumerate((positions // GRID_W, positions % GRID_W)):
        angles = coords.astype(jnp.float32)[:, None] * inverse[None, :]
        cosine = jnp.cos(angles)[:, None, :]
        sine = jnp.sin(angles)[:, None, :]
        section = values[..., axis_pos * half_dim : (axis_pos + 1) * half_dim]
        first_half = section[..., :quarter]
        second_half = section[..., quarter:]
        outputs += [
            first_half * cosine - second_half * sine,
            second_half * cosine + first_half * sine,
        ]
    return jnp.concatenate(outputs, axis=-1)


def prepare(projected, gain, positions):
    values = projected.astype(jnp.float32)
    normed = values * lax.rsqrt(jnp.mean(values * values, axis=-1, keepdims=True) + EPSILON) * gain
    return rotate(normed, positions).astype(jnp.bfloat16)


def normalize(stream, gain):
    values = stream.astype(jnp.float32)
    return (
        values * lax.rsqrt(jnp.mean(values * values, axis=-1, keepdims=True) + EPSILON) * gain
    ).astype(jnp.bfloat16)


def body(
    resid,
    query,
    key,
    value,
    q_gain,
    k_gain,
    out_weight,
    norm_gain,
    gate_weight,
    up_weight,
    down_weight,
):
    rows_here = query.shape[0]
    head_dim = q_gain.shape[0]
    heads_here = query.shape[1] // head_dim
    kv_here = key.shape[1] // head_dim
    group_size = heads_here // kv_here
    score_scale = head_dim ** (-0.5)
    positions = lax.axis_index("sp") * rows_here + jnp.arange(rows_here, dtype=jnp.int32)
    q_rot = prepare(query.reshape(rows_here, heads_here, head_dim), q_gain, positions)
    k_rot = prepare(key.reshape(rows_here, kv_here, head_dim), k_gain, positions)
    val_rows = value.reshape(rows_here, kv_here, head_dim)
    grouped = q_rot.reshape(rows_here, kv_here, group_size, head_dim)

    def key_block(carry, block):
        maxima, totals, accum = carry
        block_keys, block_vals = block
        scores = (
            jnp.einsum("qkgd,skd->kgqs", grouped, block_keys, preferred_element_type=jnp.float32)
            * score_scale
        )
        new_max = jnp.maximum(maxima, jnp.max(scores, axis=-1))
        shrink = jnp.exp(maxima - new_max)
        weights = jnp.exp(scores - new_max[..., None])
        totals = totals * shrink + jnp.sum(weights, axis=-1)
        accum = accum * shrink[..., None] + jnp.einsum(
            "kgqs,skd->kgqd",
            weights.astype(jnp.bfloat16),
            block_vals,
            preferred_element_type=jnp.float32,
        )
        return ((new_max, totals, accum), None)

    start_max = jnp.full((kv_here, group_size, rows_here), -1e30, jnp.float32)
    start_total = jnp.zeros((kv_here, group_size, rows_here), jnp.float32)
    start_accum = jnp.zeros((kv_here, group_size, rows_here, head_dim), jnp.float32)
    carry = (start_max, start_total, start_accum)
    key_part = lax.all_gather(k_rot, "sp", axis=0, tiled=True)
    val_part = lax.all_gather(val_rows, "sp", axis=0, tiled=True)
    length = key_part.shape[0]
    factor = 4
    span = rows_here * factor
    turns = length // span
    key_blocks = key_part.reshape(turns, span, kv_here, head_dim)
    val_blocks = val_part.reshape(turns, span, kv_here, head_dim)
    carry, _ = lax.scan(key_block, carry, (key_blocks, val_blocks))
    maxima, totals, accum = carry
    attn = (
        jnp.transpose(accum / totals[..., None], (2, 0, 1, 3))
        .reshape(rows_here, heads_here * head_dim)
        .astype(jnp.bfloat16)
    )
    share = rows_here // lax.axis_size("tp")
    my_first = lax.axis_index("tp") * share
    proj = lax.psum_scatter(
        jnp.dot(attn, out_weight, preferred_element_type=jnp.float32).astype(jnp.bfloat16),
        "tp",
        scatter_dimension=0,
        tiled=True,
    ).astype(jnp.float32)
    my_resid = lax.dynamic_slice_in_dim(resid, my_first, share, 0)
    my_stream = (my_resid.astype(jnp.float32) + proj).astype(jnp.bfloat16)
    mixer_rows = lax.all_gather(normalize(my_stream, norm_gain), "tp", axis=0, tiled=True)

    def add_rows(shard_rows):
        return jnp.dot(mixer_rows, shard_rows, preferred_element_type=jnp.float32)

    gate = add_rows(lax.all_gather(gate_weight, "sp", axis=0, tiled=True))
    up_part = add_rows(lax.all_gather(up_weight, "sp", axis=0, tiled=True))
    hidden = (jax.nn.silu(gate) * up_part).astype(jnp.bfloat16)
    down_whole = lax.all_gather(down_weight, "sp", axis=1, tiled=True)
    down = lax.psum_scatter(
        jnp.dot(hidden, down_whole, preferred_element_type=jnp.float32).astype(jnp.bfloat16),
        "tp",
        scatter_dimension=0,
        tiled=True,
    ).astype(jnp.float32)
    return (my_stream.astype(jnp.float32) + 0.5 * down).astype(jnp.bfloat16)


def solution(mesh):
    placed = (
        P("sp", None),
        P("sp", "tp"),
        P("sp", "tp"),
        P("sp", "tp"),
        P(),
        P(),
        P("tp", None),
        P(),
        P("sp", "tp"),
        P("sp", "tp"),
        P("tp", "sp"),
    )
    return jax.shard_map(
        body, mesh=mesh, in_specs=placed, out_specs=P(("sp", "tp"), None), check_vma=False
    )
```

profile of v0, /device:TPU:0, one launch (start us, length us, event | category | flops | bytes accessed | tf_op | source)
XLA Modules:
  0.0 702.4 jit_solution(25329568361684075)
XLA Ops:
  15.1 67.4 %all-gather.6.cloned.1.call-done = bf16[3072,4,128]{2,1,0:T(4,128)(2,1)} async-done(((bf16[192,4,128]{2,1,0:T(4,128)(2,1)}), bf16[3072,4,128]{2,1,0:T(4,128)(2,1)}) %all-gather.6.cloned.1.call-update) | async-done | bytes 3145744 | tf_op jit(solution)/shard_map/all_gather | solution.py:91
  82.5 69.2 %all-gather.8.cloned.1.call-done = bf16[3072,4,128]{2,1,0:T(4,128)(2,1)} async-done(((bf16[192,4,128]{2,1,0:T(4,128)(2,1)}), bf16[3072,4,128]{2,1,0:T(4,128)(2,1)}) %all-gather.8.cloned.1.call-update) | async-done | bytes 3145744 | tf_op jit(solution)/shard_map/all_gather | solution.py:92
  151.7 40.1 %while.15 = (s32[]{:T(128)}, f32[4,2,192]{2,1,0:T(2,128)S(1)}, f32[4,2,192]{2,1,0:T(2,128)S(1)}, f32[4,2,192,128]{3,2,1,0:T(8,128)S(1)}, bf16[4,768,4,128]{3,2,1...) while((s32[]{:T(128)}, f32[4,2,192]{2,1,0:T(2,128)S(1)}, ...), condition=%wide.region_5.6_spmd.clone, body=%wide.region_2.5_spmd.clone.sunk | while | flops 614014464 | bytes 39813256 | solution.py:99
  151.7 1.9 constant_dynamic-slice_fusion.3
  153.6 2.9 bitcast_reduce_fusion.2
  156.5 3.5 fusion.42
  161.7 1.9 constant_dynamic-slice_fusion.3
  163.6 2.9 bitcast_reduce_fusion.2
  166.6 3.5 fusion.42
  171.7 1.9 constant_dynamic-slice_fusion.3
  173.6 2.9 bitcast_reduce_fusion.2
  176.6 3.5 fusion.42
  181.7 1.9 constant_dynamic-slice_fusion.3
  183.7 2.9 bitcast_reduce_fusion.2
  186.6 3.5 fusion.42
  192.8 4.1 convolution_convert_fusion.1
  198.7 5.1 reduce-scatter.3.cloned.1.call-done
  205.2 2.5 all_gather.20
  207.7 141.2 %all-gather.10.cloned.1.call-done = bf16[2048,2816]{1,0:T(8,128)(2,1)} async-done(((bf16[128,2816]{1,0:T(8,128)(2,1)}), bf16[2048,2816]{1,0:T(8,128)(2,1)}) %all-gather.10.cloned.1.call-update) | async-done | bytes 11534352 | tf_op jit(solution)/shard_map/all_gather | solution.py:121
  348.9 6.7 fusion.24
  355.6 135.6 %all-gather.12.cloned.1.call-done = bf16[2048,2816]{1,0:T(8,128)(2,1)} async-done(((bf16[128,2816]{1,0:T(8,128)(2,1)}), bf16[2048,2816]{1,0:T(8,128)(2,1)}) %all-gather.12.cloned.1.call-update) | async-done | bytes 11534352 | tf_op jit(solution)/shard_map/all_gather | solution.py:122
  491.2 182.8 %all-gather.14.cloned.1.call-done = bf16[2816,2048]{1,0:T(8,128)(2,1)} async-done(((bf16[2816,128]{1,0:T(8,128)(2,1)}), bf16[2816,2048]{1,0:T(8,128)(2,1)}) %all-gather.14.cloned.1.call-update) | async-done | bytes 11534352 | tf_op jit(solution)/shard_map/all_gather | solution.py:124
  674.0 13.2 %convolution_convert_fusion = bf16[192,2048]{1,0:T(8,128)(2,1)} fusion(bf16[2816,2048]{1,0:T(8,128)(2,1)} %all-gather.14.cloned.1.call-done, bf16[192,2048]{1,0:T(8,128)(2,1)S(1)} %all_gather.20, bf16[2048,2816]{1,0:T(8,128)(2,1)} %all-gather.12.cloned.1.call-done, f32[192,2816]{1,0:T(8,128)S(1)} %fusion.24), kind=kOutput, calls=%fused_computation.23 | convolution fusion | flops 4432822272 | bytes 26804224 | tf_op jit(solution)/shard_map/dot_general | solution.py:126
  687.2 6.5 reduce-scatter.5.cloned.1.call-done
  (81 shorter events, 20.8 us)
Async XLA Ops:
  6.5 5.2 copy-start.2
  6.5 6.1 copy-start.1
  6.5 75.9 %all-gather.6.cloned.1.call-start = ((), (), s32[]{:S(2)}) async-start(), calls=%async_computation.2 | async-start | bytes 3342336 | tf_op jit(solution)/shard_map/all_gather | solution.py:91
  8.0 5.3 copy-start.5
  11.7 140.0 %all-gather.8.cloned.1.call-start = ((), (), s32[]{:S(2)}) async-start(), calls=%async_computation.3 | async-start | bytes 3342336 | tf_op jit(solution)/shard_map/all_gather | solution.py:92
  12.5 191.2 %reduce-scatter.3.cloned.1.call-start = ((), (), s32[]{:S(2)}) async-start(), calls=%async_computation.4 | async-start | bytes 1179648 | tf_op jit(solution)/shard_map/reduce_scatter | solution.py:108
  156.5 3.8 copy-start
  166.5 3.8 copy-start
  176.6 3.8 copy-start
  186.6 3.8 copy-start
  192.5 11.3 %copy-start.3 = (bf16[192,2048]{1,0:T(8,128)(2,1)S(1)}, bf16[192,2048]{1,0:T(8,128)(2,1)}, u32[]{:S(2)}) copy-start(bf16[192,2048]{1,0:T(8,128)(2,1)} %param.13) | copy-start | bytes 2359300
  192.7 12.3 %copy-start.4 = (f32[2048]{0:T(1024)S(1)}, f32[2048]{0:T(1024)}, u32[]{:S(2)}) copy-start(f32[2048]{0:T(1024)} %param.20) | copy-start | bytes 24580
  196.9 152.0 %all-gather.10.cloned.1.call-start = ((), (), s32[]{:S(2)}) async-start(), calls=%async_computation.5 | async-start | bytes 12255232 | tf_op jit(solution)/shard_map/all_gather | solution.py:121
  197.5 293.7 %all-gather.12.cloned.1.call-start = ((), (), s32[]{:S(2)}) async-start(), calls=%async_computation.6 | async-start | bytes 12255232 | tf_op jit(solution)/shard_map/all_gather | solution.py:122
  198.1 475.9 %all-gather.14.cloned.1.call-start = ((), (), s32[]{:S(2)}) async-start(), calls=%async_computation.7 | async-start | bytes 12255232 | tf_op jit(solution)/shard_map/all_gather | solution.py:124
  198.6 495.1 %reduce-scatter.5.cloned.1.call-start = ((), (), s32[]{:S(2)}) async-start(), calls=%async_computation.8 | async-start | bytes 1179648 | tf_op jit(solution)/shard_map/reduce_scatter | solution.py:125
Sparse Core Ops, SparseCore 0:
  11.9 70.5 all-gather.5
  85.2 66.3 all-gather.7
  197.0 6.6 reduce-scatter.2
  206.4 142.5 all-gather.9
  351.5 139.5 all-gather.11
  493.7 180.2 all-gather.13
  687.3 6.3 reduce-scatter.4
where the time goes:
time: 703 us; the launch traced here: 702 us
  waiting for transfers between devices  609 us (87%)
  matrix products  41.2 us (6%)
  other arithmetic  23.7 us (3%)
  between operations  13.8 us (2%)
  local copies, waits for them, and re-layouts  11.4 us (2%)
    all_gather x1, waiting for transfers between devices, body(): down_whole = lax.all_gather(down_weight, 'sp', axis=1, tiled=True)  183 us
    all_gather x1, waiting for transfers between devices, body(): gate = add_rows(lax.all_gather(gate_weight, 'sp', axis=0, tiled=True))  141 us
    all_gather x1, waiting for transfers between devices, body(): up_part = add_rows(lax.all_gather(up_weight, 'sp', axis=0, tiled=True))  136 us
    all_gather x1, waiting for transfers between devices, body(): val_part = lax.all_gather(val_rows, 'sp', axis=0, tiled=True)  69.2 us
    all_gather x1, waiting for transfers between devices, body(): key_part = lax.all_gather(k_rot, 'sp', axis=0, tiled=True)  67.4 us
    reduce_sum x4, other arithmetic, key_block(): totals = totals * shrink + jnp.sum(weights, axis=-1)  14.2 us
  transfers between devices with their start and end apart: 7, of which 7 were waited for; matrix products, arithmetic and copies ran while one was open for 2% of the time, Pallas kernels for 0%

commit v1 on v0

--- a/solution.py
+++ b/solution.py
@@ -5,6 +5,14 @@
 
 GRID_W = 64
 EPSILON = 1e-06
+
+
+def reach_target(my_tile, point, along_axis):
+    return jnp.split(
+        lax.all_gather(jnp.concatenate([my_tile, point], axis=1), along_axis, axis=0, tiled=True),
+        [my_tile.shape[1]],
+        axis=1,
+    )
 
 
 def rotate(values, positions):
@@ -88,8 +96,7 @@
     start_total = jnp.zeros((kv_here, group_size, rows_here), jnp.float32)
     start_accum = jnp.zeros((kv_here, group_size, rows_here, head_dim), jnp.float32)
     carry = (start_max, start_total, start_accum)
-    key_part = lax.all_gather(k_rot, "sp", axis=0, tiled=True)
-    val_part = lax.all_gather(val_rows, "sp", axis=0, tiled=True)
+    key_part, val_part = reach_target(k_rot, val_rows, "sp")
     length = key_part.shape[0]
     factor = 4
     span = rows_here * factor

time: 703 us -> 673 us (0.957)
  waiting for transfers between devices: 609 us -> 567 us
  matrix products: 41.2 us -> 49.7 us
    all_gather x2 -> x1, waiting for transfers between devices: 137 us -> 93.7 us  [reach_target(): lax.all_gather(jnp.concatenate([my_tile, point], axis=1), along_axis, axi...]
    dynamic_slice x4 -> x0, local copies, waits for them, and re-layouts: 7.66 us -> none  [body(): carry, _ = lax.scan(key_block, carry, (key_blocks, val_blocks))]
    split x0 -> x1, local copies, waits for them, and re-layouts: none -> 7.09 us  [reach_target(): jnp.split(lax.all_gather(jnp.concatenate([my_tile, point], axis=1), along...]
  transfers between devices with their start and end apart: 7 -> 6, of which waited for: 7 -> 6; matrix products, arithmetic and copies ran while one was open for 2% -> 2% of each run, Pallas kernels for 0% -> 0%
where the time goes in v1:
time: 673 us; the launch traced here: 672 us
  waiting for transfers between devices  567 us (84%)
  matrix products  49.7 us (7%)
  other arithmetic  23.9 us (4%)
  local copies, waits for them, and re-layouts  15.3 us (2%)
  between operations  13.7 us (2%)
    all_gather x1, waiting for transfers between devices, body(): down_whole = lax.all_gather(down_weight, 'sp', axis=1, tiled=True)  176 us
    all_gather x1, waiting for transfers between devices, body(): up_part = add_rows(lax.all_gather(up_weight, 'sp', axis=0, tiled=True))  142 us
    all_gather x1, waiting for transfers between devices, body(): gate = add_rows(lax.all_gather(gate_weight, 'sp', axis=0, tiled=True))  142 us
    all_gather x1, waiting for transfers between devices, reach_target(): lax.all_gather(jnp.concatenate([my_tile, point], axis=1), along_axis, axi...  93.7 us
    dot_general x4, matrix products, key_block(): jnp.einsum('qkgd,skd->kgqs', grouped, block_keys, preferred_element_type=...  16.2 us
    reduce_sum x4, other arithmetic, key_block(): totals = totals * shrink + jnp.sum(weights, axis=-1)  14.2 us
  transfers between devices with their start and end apart: 6, of which 6 were waited for; matrix products, arithmetic and copies ran while one was open for 2% of the time, Pallas kernels for 0%

profile of v1, /device:TPU:0, one launch (start us, length us, event | category | flops | bytes accessed | tf_op | source)
XLA Modules:
  0.0 672.1 jit_solution(14385280073637313155)
XLA Ops:
  15.5 93.7 %all-gather.5.cloned.1.call-done = bf16[3072,8,128]{2,1,0:T(8,128)(2,1)} async-done(((bf16[192,8,128]{2,1,0:T(8,128)(2,1)}), bf16[3072,8,128]{2,1,0:T(8,128)(2,1)}) %all-gather.5.cloned.1.call-update) | async-done | bytes 6291472 | tf_op jit(solution)/shard_map/all_gather | solution.py:12
  109.2 7.1 %fusion.30 = (bf16[3072,4,128]{2,1,0:T(4,128)(2,1)S(1)}, bf16[3072,4,128]{2,1,0:T(4,128)(2,1)S(1)}) fusion(bf16[3072,8,128]{2,1,0:T(8,128)(2,1)} %all-gather.5.cloned.1.call-done), kind=kLoop, calls=%fused_computation.71 | loop fusion | bytes 12582912 | tf_op jit(solution)/shard_map/split | solution.py:11
  120.5 40.8 %while.15 = (s32[]{:T(128)}, f32[4,2,192]{2,1,0:T(2,128)S(1)}, f32[4,2,192]{2,1,0:T(2,128)S(1)}, f32[4,2,192,128]{3,2,1,0:T(8,128)S(1)}, bf16[4,768,4,128]{3,1,0...) while((s32[]{:T(128)}, f32[4,2,192]{2,1,0:T(2,128)S(1)}, ...), condition=%wide.region_5.6_spmd.clone, body=%wide.region_2.5_spmd.clone.sunk | while | flops 614014464 | bytes 36668548 | solution.py:106
  120.5 4.0 bitcast_reduce_fusion.2
  124.5 3.5 fusion.51
  128.3 2.4 fusion.53
  130.7 4.1 bitcast_reduce_fusion.2
  134.7 3.5 fusion.51
  138.5 2.4 fusion.53
  140.9 4.1 bitcast_reduce_fusion.2
  145.0 3.5 fusion.51
  148.7 2.4 fusion.53
  151.1 4.1 bitcast_reduce_fusion.2
  155.2 3.5 fusion.51
  158.9 2.4 fusion.53
  162.3 4.1 convolution_convert_fusion.1
  168.6 4.7 reduce-scatter.3.cloned.1.call-done
  174.7 2.4 all_gather.16
  177.1 141.5 %all-gather.7.cloned.1.call-done = bf16[2048,2816]{1,0:T(8,128)(2,1)} async-done(((bf16[128,2816]{1,0:T(8,128)(2,1)}), bf16[2048,2816]{1,0:T(8,128)(2,1)}) %all-gather.7.cloned.1.call-update) | async-done | bytes 11534352 | tf_op jit(solution)/shard_map/all_gather | solution.py:128
  318.6 6.7 fusion.31
  325.3 176.1 %all-gather.11.cloned.1.call-done = bf16[2816,2048]{1,0:T(8,128)(2,1)} async-done(((bf16[2816,128]{1,0:T(8,128)(2,1)}), bf16[2816,2048]{1,0:T(8,128)(2,1)}) %all-gather.11.cloned.1.call-update) | async-done | bytes 11534352 | tf_op jit(solution)/shard_map/all_gather | solution.py:131
  501.4 142.2 %all-gather.9.cloned.1.call-done = bf16[2048,2816]{1,0:T(8,128)(2,1)} async-done(((bf16[128,2816]{1,0:T(8,128)(2,1)}), bf16[2048,2816]{1,0:T(8,128)(2,1)}) %all-gather.9.cloned.1.call-update) | async-done | bytes 11534352 | tf_op jit(solution)/shard_map/all_gather | solution.py:129
  643.7 13.2 %convolution_convert_fusion = bf16[192,2048]{1,0:T(8,128)(2,1)} fusion(bf16[2816,2048]{1,0:T(8,128)(2,1)} %all-gather.11.cloned.1.call-done, bf16[192,2048]{1,0:T(8,128)(2,1)S(1)} %all_gather.16, bf16[2048,2816]{1,0:T(8,128)(2,1)} %all-gather.9.cloned.1.call-done, f32[192,2816]{1,0:T(8,128)S(1)} %fusion.31), kind=kOutput, calls=%fused_computation.25 | convolution fusion | flops 4432822272 | bytes 26804224 | tf_op jit(solution)/shard_map/dot_general | solution.py:133
  656.9 6.5 reduce-scatter.5.cloned.1.call-done
  (75 shorter events, 20.1 us)
Async XLA Ops:
  6.5 6.4 copy-start.1
  6.5 102.6 %all-gather.5.cloned.1.call-start = ((), (), s32[]{:S(2)}) async-start(), calls=%async_computation.2 | async-start | bytes 6684672 | tf_op jit(solution)/shard_map/all_gather | solution.py:12
  9.0 4.7 copy-start.4
  12.9 160.4 %reduce-scatter.3.cloned.1.call-start = ((), (), s32[]{:S(2)}) async-start(), calls=%async_computation.3 | async-start | bytes 1179648 | tf_op jit(solution)/shard_map/reduce_scatter | solution.py:115
  124.5 3.8 copy-start
  134.7 3.8 copy-start
  144.9 3.8 copy-start
  155.2 3.8 copy-start
  162.0 11.3 %copy-start.2 = (bf16[192,2048]{1,0:T(8,128)(2,1)S(1)}, bf16[192,2048]{1,0:T(8,128)(2,1)}, u32[]{:S(2)}) copy-start(bf16[192,2048]{1,0:T(8,128)(2,1)} %param.13) | copy-start | bytes 2359300
  162.3 12.3 %copy-start.3 = (f32[2048]{0:T(1024)S(1)}, f32[2048]{0:T(1024)}, u32[]{:S(2)}) copy-start(f32[2048]{0:T(1024)} %param.20) | copy-start | bytes 24580
  166.4 152.2 %all-gather.7.cloned.1.call-start = ((), (), s32[]{:S(2)}) async-start(), calls=%async_computation.4 | async-start | bytes 12255232 | tf_op jit(solution)/shard_map/all_gather | solution.py:128
  167.2 334.3 %all-gather.11.cloned.1.call-start = ((), (), s32[]{:S(2)}) async-start(), calls=%async_computation.6 | async-start | bytes 12255232 | tf_op jit(solution)/shard_map/all_gather | solution.py:131
  167.8 475.9 %all-gather.9.cloned.1.call-start = ((), (), s32[]{:S(2)}) async-start(), calls=%async_computation.5 | async-start | bytes 12255232 | tf_op jit(solution)/shard_map/all_gather | solution.py:129
  168.3 495.1 %reduce-scatter.5.cloned.1.call-start = ((), (), s32[]{:S(2)}) async-start(), calls=%async_computation.7 | async-start | bytes 1179648 | tf_op jit(solution)/shard_map/reduce_scatter | solution.py:132
Sparse Core Ops, SparseCore 0:
  13.0 96.1 all-gather.4
  166.6 6.6 reduce-scatter.2
  176.1 142.5 all-gather.6
  321.2 180.2 all-gather.10
  504.0 139.5 all-gather.8
  657.0 6.3 reduce-scatter.4
